TPU v7x, 32 devices: a whole 2x2x4 slice. The times are simulated.
32 devices in a mesh: gr: 2 (over y), fs: 4 (over z), tp: 4 (over x, core).
Axes of the slice: x: 2, y: 2, z: 4, core: 2. Of those that a mesh axis runs over, the one named last changes fastest.
Arguments:
- prompt: bfloat16 [4096, 2048], P(('gr', 'fs')), may hold values from -6 to 6
- norm_gain: float32 [2048], P(('gr', 'fs')), may hold values from 0.1 to 1.9
- gate_master: float32 [32, 2048, 1024], P(None, ('gr', 'fs'), 'tp'), may hold values from -6 to 6
- up_master: float32 [32, 2048, 1024], P(None, ('gr', 'fs'), 'tp'), may hold values from -6 to 6
- down_master: float32 [32, 2048, 1024], P(None, ('gr', 'fs'), 'tp'), may hold values from -6 to 6
- routes: int32 [4096, 2], P(('gr', 'fs')), may hold values from 0 to 31, as said below
- route_weights: float32 [4096, 2], P(('gr', 'fs')), may hold values from 0.1 to 0.9
Outputs:
- gate_ready: bfloat16 [32, 2048, 1024], P('fs', None, 'tp')
- up_ready: bfloat16 [32, 2048, 1024], P('fs', None, 'tp')
- down_ready: bfloat16 [32, 2048, 1024], P('fs', None, 'tp')
- blended: bfloat16 [4096, 2048], P(('gr', 'fs'), 'tp')
Inputs may be any that keep to these rules, and one draw needn't show every extreme that they name: `routes`: each row names 2 different experts of one group: expert // 8 is the group. In every aligned block of 512 rows (the tokens of one index of gr and fs) half of the rows choose one group, and no expert is named more than 64 times; in every block some expert is named exactly 64 times.
All inputs are finite; a program needn't handle non-finite values.
Results may differ from a plain program's by a relative error of at most 0.015.
Values may be sent and summed in bfloat16 or wider, within the bound.
A program may use at most 128 MiB of HBM per device.

v0:
```python
import functools

import jax
import jax.numpy as jnp
from jax import lax
from jax.experimental import pallas as pl
from jax.experimental.pallas import tpu as pltpu
from jax.sharding import PartitionSpec as P

EPS = 1e-06
GROUP = 8
MESH = pl.DeviceIdType.MESH
STEPS = ((0, 0), (1, 0), (0, 1), (1, 1), (2, 0), (2, 1))
SLOTS = 4


def kernel(
    dims, gain, gm, um, dm, tok, wsend, g_out, u_out, d_out, ans,
    stage, wb, x, w, gb, ub, db, hid, yr, ys,
    st_sem, zs, zr, vs, vr, own_sem, tzs, tzr, wzs, wzr, txs, txr, tw_sem, ld_sem, dl_sem,
    ps, pr, rs, rr, rl_sem,
):
    gr, fs, tp, experts, rows, width, cap, depth, hidden_all = dims
    me_g, me_f, me_t = lax.axis_index("gr"), lax.axis_index("fs"), lax.axis_index("tp")
    local = experts // fs
    half = local // 2
    quarter = depth // tp
    total = fs * cap
    tile = min(256, cap)
    piece_rows = max(rows, 128)
    per_owner = quarter // piece_rows
    masters, outs = (gm, um, dm), (g_out, u_out, d_out)

    def fs_at(k):
        return lax.rem(me_f + k, fs)

    def fs_from(k):
        return lax.rem(me_f + fs - k, fs)

    def gr_at(j):
        return lax.rem(me_g + j, gr)

    def remote(src, dst, ssem, rsem, where):
        return pltpu.make_async_remote_copy(
            src_ref=src, dst_ref=dst, send_sem=ssem, recv_sem=rsem,
            device_id=where, device_id_type=MESH,
        )

    def region(s, g, f):
        m, h = STEPS[s]
        at = pl.multiple_of((g * fs + f) * rows, rows)
        return outs[m].at[pl.ds(h * half, half), pl.ds(at, rows), :]

    barrier = pltpu.get_barrier_semaphore()
    for k in range(1, fs):
        pl.semaphore_signal(barrier, inc=1, device_id={"fs": fs_at(k)}, device_id_type=MESH)
    for j in range(1, gr):
        pl.semaphore_signal(barrier, inc=1, device_id={"gr": gr_at(j)}, device_id_type=MESH)
    for j in range(1, tp):
        pl.semaphore_signal(
            barrier, inc=1, device_id={"tp": lax.rem(me_t + j, tp)}, device_id_type=MESH
        )
    pl.semaphore_wait(barrier, (fs - 1) + (gr - 1) + (tp - 1))

    def x_block(f, t):
        return x.at[
            pl.ds(pl.multiple_of(f * cap, cap), cap),
            pl.ds(pl.multiple_of(t * quarter, quarter), quarter),
        ]

    def w_block(f):
        return w.at[:, pl.ds(pl.multiple_of(f * cap, cap), cap)]

    if fs == 4:
        odd, side = lax.rem(me_f, 2), lax.rem(me_t, 2)
        near, far = 1 + 2 * odd, 3 - 2 * odd
        sending = [
            jnp.where(side == 0, 2, near), jnp.where(side == 0, far, 2), jnp.where(side == 0, near, far)
        ]
        hearing = [2, 1, 3]
    else:
        sending = list(range(1, fs))
        hearing = sending
    items = [(s, k) for s in range(4) for k in [0] + sending]
    items += [(s, k) for k in [0] + sending for s in (4, 5)]

    def load(i):
        s, k = items[i]
        m, h = STEPS[s]
        return pltpu.make_async_copy(
            masters[m].at[pl.ds(fs_at(k) * local + h * half, half)],
            stage.at[i % SLOTS], st_sem.at[i % SLOTS],
        )

    for i in range(SLOTS):
        load(i).start()

    sends = []
    early = []
    for k in range(1, fs):
        dst = fs_at(k)
        c = remote(tok.at[(dst * local) // GROUP], x_block(me_f, me_t), tzs.at[k], tzr.at[k], {"fs": dst})
        c.start()
        sends.append(c)
        c = remote(wsend.at[dst], w_block(me_f), wzs.at[k], wzr.at[k], {"fs": dst})
        c.start()
        sends.append(c)
    own_tok = pltpu.make_async_copy(
        tok.at[(me_f * local) // GROUP], x_block(me_f, me_t), tw_sem.at[0]
    )
    own_tok.start()
    own_w = pltpu.make_async_copy(wsend.at[me_f], w_block(me_f), tw_sem.at[1])
    own_w.start()

    own_copies = {}

    def send_gr(s, k, src):
        f = fs_from(k)
        for j in range(1, gr):
            c = remote(src, region(s, me_g, f), vs.at[s, k, j - 1], vr.at[s, k, j - 1], {"gr": gr_at(j)})
            c.start()
            sends.append(c)

    for i, (s, k) in enumerate(items):
        m, h = STEPS[s]
        load(i).wait()

        def cast(e, carry, s=s, k=k, m=m, i=i):
            value = stage[i % SLOTS, e]
            if m < 2:
                value = gain[...] * value
            wb[s, k, e] = value.astype(jnp.bfloat16)
            return carry

        lax.fori_loop(0, half, cast, 0)
        if i + SLOTS < len(items):
            load(i + SLOTS).start()
        if isinstance(k, int) and k == 0:
            c = pltpu.make_async_copy(wb.at[s, 0], region(s, me_g, me_f), own_sem.at[s])
            c.start()
            own_copies[s] = c
            if m < 2:
                send_gr(s, 0, wb.at[s, 0])
        else:
            c = remote(wb.at[s, k], region(s, me_g, me_f), zs.at[s, k], zr.at[s, k], {"fs": fs_at(k)})
            c.start()
            sends.append(c)

    own_tok.wait()
    own_w.wait()
    for k in range(fs):
        f = fs_from(k)
        if k > 0:
            remote(x_block(f, me_t), x_block(f, me_t), tzs.at[k], tzr.at[k], {"fs": f}).wait_recv()
            remote(w_block(f), w_block(f), wzs.at[k], wzr.at[k], {"fs": f}).wait_recv()
        for j in range(1, tp):
            c = remote(
                x_block(f, me_t), x_block(f, me_t), txs.at[k, j], txr.at[k, j],
                {"tp": lax.rem(me_t + j, tp)},
            )
            c.start()
            early.append(c)

    def forward(s, k):
        f = fs_from(k)
        remote(region(s, me_g, f), region(s, me_g, f), zs.at[s, k], zr.at[s, k], {"fs": f}).wait_recv()
        send_gr(s, k, region(s, me_g, f))

    def arrived_gr(s, k):
        f = fs_from(k)
        for j in range(1, gr):
            g = lax.rem(me_g + gr - j, gr)
            remote(
                region(s, g, f), region(s, g, f), vs.at[s, k, j - 1], vr.at[s, k, j - 1], {"gr": g}
            ).wait_recv()

    def loads(e, slot):
        return (
            pltpu.make_async_copy(g_out.at[e], gb.at[slot], ld_sem.at[0, slot]),
            pltpu.make_async_copy(u_out.at[e], ub.at[slot], ld_sem.at[1, slot]),
        )

    def experts_of(h):
        first = h * half
        for c in loads(first, 0):
            c.start()

        def one(n, carry):
            slot = lax.rem(n, 2)
            e = first + n

            @pl.when(n + 1 < half)
            def _():
                for c in loads(e + 1, 1 - slot):
                    c.start()

            for c in loads(e, slot):
                c.wait()

            def block(r, carry):
                at = pl.ds(pl.multiple_of(r * tile, tile), tile)
                xs = x[at, :]
                pre_gate = jnp.dot(xs, gb[slot], preferred_element_type=jnp.float32) * depth ** (-0.5)
                pre_up = jnp.dot(xs, ub[slot], preferred_element_type=jnp.float32) * depth ** (-0.5)
                ws = jnp.transpose(w[:, at])
                lane = lax.broadcasted_iota(jnp.int32, ws.shape, 1)
                weight = jnp.sum(jnp.where(lane == e, ws, 0.0), axis=1, keepdims=True)
                value = pre_gate / (1.0 + jnp.exp(-pre_gate)) * pre_up * weight
                hid[e, at, :] = value.astype(jnp.bfloat16)
                return carry

            lax.fori_loop(0, total // tile, block, 0)
            return carry

        lax.fori_loop(0, half, one, 0)

    chunks = []

    def chunk(index):
        ci = len(chunks)
        at = pl.multiple_of(index * piece_rows, piece_rows)
        owner = index // per_owner
        piece = lax.rem(index, per_owner)
        slot = ci % 2
        c = pltpu.make_async_copy(d_out.at[:, pl.ds(at, piece_rows), :], db.at[slot], dl_sem.at[slot])
        c.start()
        c.wait()

        def block(r, carry):
            here = pl.ds(pl.multiple_of(r * tile, tile), tile)
            acc = jnp.zeros((tile, piece_rows), jnp.float32)
            for e in range(local):
                acc += lax.dot_general(
                    hid[e, here, :], db[slot, e], (((1,), (1,)), ((), ())),
                    preferred_element_type=jnp.float32,
                )
            x[here, pl.ds(at, piece_rows)] = (acc * hidden_all ** (-0.5)).astype(jnp.bfloat16)
            return carry

        lax.fori_loop(0, total // tile, block, 0)
        turn = lax.rem(me_t + tp - owner, tp)
        slot_of = lax.rem(turn + tp - 1, tp)
        away = turn != 0
        chunks.append((at, owner, piece, slot_of, away))

        @pl.when(away)
        def _():
            partial_copy(ci).start()

        if ci >= 2:
            finish(ci - 2)

    def answer_part(p):
        return pl.ds(pl.multiple_of(p * piece_rows, piece_rows), piece_rows)

    def answer_copy(k, p):
        f = fs_at(k)
        at = pl.ds(pl.multiple_of(f * cap, cap), cap)
        return remote(
            ys.at[at, answer_part(p)], ans.at[me_f, :, answer_part(p)],
            rs.at[k, p], rr.at[k, p], {"fs": f},
        )

    def own_answer(p):
        at = pl.ds(pl.multiple_of(me_f * cap, cap), cap)
        return pltpu.make_async_copy(
            ys.at[at, answer_part(p)], ans.at[me_f, :, answer_part(p)], rl_sem.at[p]
        )

    def finish(ci):
        here, owner, p, slot_of, away = chunks[ci]

        @pl.when(jnp.logical_not(away))
        def _():
            for j in range(1, tp):
                ref = yr.at[j - 1, :, answer_part(p)]
                remote(
                    ref, ref, ps.at[ci], pr.at[j - 1, p], {"tp": lax.rem(me_t + j, tp)}
                ).wait_recv()
            for k in list(range(1, fs)) + [0]:
                at = pl.ds(pl.multiple_of(fs_at(k) * cap, cap), cap)
                value = x[at, pl.ds(here, piece_rows)].astype(jnp.float32)
                for j in range(tp - 1):
                    value += yr[j, at, answer_part(p)].astype(jnp.float32)
                ys[at, answer_part(p)] = value.astype(jnp.bfloat16)
                if k > 0:
                    answer_copy(k, p).start()
                else:
                    own_answer(p).start()

    def partial_copy(ci):
        at, owner, piece, slot_of, away = chunks[ci]
        return remote(
            x.at[:, pl.ds(at, piece_rows)],
            yr.at[slot_of, :, pl.ds(pl.multiple_of(piece * piece_rows, piece_rows), piece_rows)],
            ps.at[ci], pr.at[slot_of, piece], {"tp": owner},
        )

    for s in (0, 1, 2):
        for k in hearing:
            forward(s, k)
    send_gr(4, 0, wb.at[4, 0])
    for k in range(fs):
        f = fs_from(k)
        for j in range(1, tp):
            t = lax.rem(me_t + tp - j, tp)
            remote(x_block(f, t), x_block(f, t), txs.at[k, j], txr.at[k, j], {"tp": t}).wait_recv()
    for s in (0, 1):
        own_copies[s].wait()
        for k in range(fs):
            arrived_gr(s, k)
    experts_of(0)
    for k in hearing:
        forward(3, k)
    send_gr(5, 0, wb.at[5, 0])
    for s in (2, 3):
        own_copies[s].wait()
        for k in range(fs):
            arrived_gr(s, k)
    experts_of(1)
    for c in early:
        c.wait_send()
    own_copies[4].wait()
    own_copies[5].wait()
    apart = rows == piece_rows

    def others(k):
        arrived_gr(4, k)
        arrived_gr(5, k)
        if apart:
            for j in range(1, gr):
                chunk(lax.rem(me_g + gr - j, gr) * fs + fs_from(k))

    if apart:
        chunk(me_g * fs + me_f)
    last = 0
    for k in hearing:
        forward(4, k)
        forward(5, k)
        if apart:
            chunk(me_g * fs + fs_from(k))
        others(last)
        last = k
    others(last)
    if not apart:
        for index in range(depth // piece_rows):
            chunk(jnp.int32(index))

    for ci in range(max(0, len(chunks) - 2), len(chunks)):
        finish(ci)
    for p in range(per_owner):
        for k in range(1, fs):
            answer_copy(k, p).wait_send()
            f = fs_from(k)
            ref = ans.at[f, :, pl.ds(p * piece_rows, piece_rows)]
            remote(ref, ref, rs.at[k, p], rr.at[k, p], {"fs": f}).wait_recv()
        own_answer(p).wait()
    for c in sends:
        c.wait_send()
    for ci in range(len(chunks)):
        @pl.when(chunks[ci][4])
        def _(ci=ci):
            partial_copy(ci).wait_send()


def per_device(prompt, norm_gain, gate_master, up_master, down_master, routes, route_weights):
    gr, fs, tp = lax.axis_size("gr"), lax.axis_size("fs"), lax.axis_size("tp")
    experts, rows, width = gate_master.shape
    tokens, depth = prompt.shape
    local = experts // fs
    half = local // 2
    groups = experts // GROUP
    cap = tokens // 2
    quarter = depth // tp
    total = fs * cap
    piece_rows = max(rows, 128)
    per_owner = quarter // piece_rows
    bf16, f32 = jnp.bfloat16, jnp.float32

    wide = prompt.astype(f32)
    scale = lax.rsqrt(jnp.mean(wide * wide, axis=-1, keepdims=True) + EPS)
    mine = lax.dynamic_slice_in_dim(prompt, lax.axis_index("tp") * quarter, quarter, 1)
    normed = (mine.astype(f32) * scale).astype(bf16)
    group = routes[:, 0] // GROUP
    hits = group[:, None] == jnp.arange(groups, dtype=jnp.int32)[None, :]
    order = jnp.arange(tokens, dtype=jnp.int32)
    before = (order[None, :] < order[:, None]).astype(bf16)
    counts = jnp.dot(before, hits.astype(bf16), preferred_element_type=f32)
    rank = jnp.sum(jnp.where(hits, counts, 0.0), axis=1).astype(jnp.int32)
    slot = group * cap + rank
    place = jnp.arange(groups * cap, dtype=jnp.int32)[:, None] == slot[None, :]
    packed = jnp.dot(place.astype(bf16), normed, preferred_element_type=f32).astype(bf16)
    packed = packed.reshape(groups, cap, quarter)
    named = jnp.arange(experts, dtype=jnp.int32)
    weights = jnp.sum(
        jnp.where(routes[:, :, None] == named[None, None, :], route_weights[:, :, None], 0.0), axis=1
    )
    packed_w = jnp.dot(place.astype(f32), weights, precision=lax.Precision.HIGHEST)
    packed_w = packed_w.reshape(groups, cap, experts)
    sent_w = jnp.stack(
        [
            jnp.pad(
                packed_w[(d * local) // GROUP, :, d * local : (d + 1) * local],
                ((0, 0), (0, max(8, local) - local)),
            ).T
            for d in range(fs)
        ]
    )
    dims = (gr, fs, tp, experts, rows, width, cap, depth, width * tp)
    any_spec = pl.BlockSpec(memory_space=pl.ANY)
    ready = jax.ShapeDtypeStruct((local, gr * fs * rows, width), bf16)
    steps = len(STEPS)
    dma = pltpu.SemaphoreType.DMA
    gate_ready, up_ready, down_ready, answers = pl.pallas_call(
        functools.partial(kernel, dims),
        name="reshard_experts",
        out_shape=(ready, ready, ready, jax.ShapeDtypeStruct((fs, cap, quarter), bf16)),
        in_specs=[pl.BlockSpec(memory_space=pltpu.VMEM)] + [any_spec] * 5,
        out_specs=(any_spec,) * 4,
        scratch_shapes=[
            pltpu.VMEM((SLOTS, half, rows, width), f32),
            pltpu.VMEM((steps, fs, half, rows, width), bf16),
            pltpu.VMEM((total, depth), bf16),
            pltpu.VMEM((max(8, local), total), f32),
            pltpu.VMEM((2, depth, width), bf16),
            pltpu.VMEM((2, depth, width), bf16),
            pltpu.VMEM((2, local, piece_rows, width), bf16),
            pltpu.VMEM((local, total, width), bf16),
            pltpu.VMEM((tp - 1, total, quarter), bf16),
            pltpu.VMEM((total, quarter), bf16),
            dma((SLOTS,)),
            dma((steps, fs)), dma((steps, fs)),
            dma((steps, fs, gr - 1)), dma((steps, fs, gr - 1)),
            dma((steps,)),
            dma((fs,)), dma((fs,)), dma((fs,)), dma((fs,)),
            dma((fs, tp)), dma((fs, tp)),
            dma((2,)),
            dma((2, 2)), dma((2,)),
            dma((tp * per_owner,)), dma((tp - 1, per_owner)),
            dma((fs, per_owner)), dma((fs, per_owner)), dma((per_owner,)),
        ],
        compiler_params=pltpu.CompilerParams(
            collective_id=0, has_side_effects=True, vmem_limit_bytes=66000000
        ),
    )(norm_gain[:, None], gate_master, up_master, down_master, packed, sent_w)
    answers = answers.reshape(groups, fs // groups, cap, quarter)
    answers = jnp.sum(answers.astype(f32), axis=1).astype(bf16).reshape(groups * cap, quarter)
    back = (slot[:, None] == jnp.arange(groups * cap, dtype=jnp.int32)[None, :]).astype(bf16)
    blended = jnp.dot(back, answers, preferred_element_type=f32)
    return (gate_ready, up_ready, down_ready, blended.astype(bf16))


def solution(mesh):
    both = ("gr", "fs")
    in_specs = (
        P(both, None),
        P(both),
        P(None, both, "tp"),
        P(None, both, "tp"),
        P(None, both, "tp"),
        P(both, None),
        P(both, None),
    )
    out_specs = (
        P("fs", None, "tp"),
        P("fs", None, "tp"),
        P("fs", None, "tp"),
        P(both, "tp"),
    )
    return jax.shard_map(
        per_device, mesh=mesh, in_specs=in_specs, out_specs=out_specs, check_vma=False
    )
```

profile of v0, /device:TPU:13, one launch (start us, length us, event | category | flops | bytes accessed | tf_op | source)
XLA Modules:
  0.0 436.3 jit_solution(12379699192008056385)
XLA Ops:
  0.6 0.0 copy-start
  0.6 0.7 and_select_fusion
  1.3 0.3 fusion.6
  1.6 0.7 select_reduce_fusion
  2.4 1.1 fusion.2
  3.5 0.6 pad_maximum_fusion.wsend
  4.1 2.1 multiply_reduce_fusion
  6.2 2.8 fusion.4
  9.0 0.0 copy-done
  9.0 0.8 copy.16.gain
  9.8 401.8 %reshard_experts.1 = (bf16[8,2048,256]{2,1,0:T(8,128)(2,1)}, bf16[8,2048,256]{2,1,0:T(8,128)(2,1)}, bf16[8,2048,256]{2,1,0:T(8,128)(2,1)}, bf16[4,256,512]{2,1,0:T(8,128)(2,1)}) custom-call(f32[256,1]{1,0:T(8,128)} %copy.16.gain, f32[32,256,256]{2,1,0:T(8,128)} %gm.1, f32[32,256,256]{2,1,0:T(8,128)} %um.1, f32[32,256,256]{2,1,0:T(8,128)} %dm.1, ...), custom_call_target="tpu_custom_call" | custom-call | tf_op jit(solution)/shard_map/reshard_experts/pallas_call | solution.py:414
  411.6 2.8 fusion.5
  414.4 7.3 %copy.20 = bf16[8,2048,256]{2,1,0:T(8,128)(2,1)} copy(bf16[8,2048,256]{2,1,0:T(8,128)(2,1)} %get-tuple-element.22) | data formatting | bytes 16777216
  421.7 7.3 %copy.21 = bf16[8,2048,256]{2,1,0:T(8,128)(2,1)} copy(bf16[8,2048,256]{2,1,0:T(8,128)(2,1)} %get-tuple-element.23) | data formatting | bytes 16777216
  429.0 7.3 %copy.22 = bf16[8,2048,256]{2,1,0:T(8,128)(2,1)} copy(bf16[8,2048,256]{2,1,0:T(8,128)(2,1)} %get-tuple-element.24) | data formatting | bytes 16777216
  (6 shorter events, 0.0 us)
Async XLA Ops:
  0.6 8.4 %copy-start = (f32[256]{0:T(256)S(1)}, f32[256]{0:T(256)}, u32[]{:S(2)}) copy-start(f32[256]{0:T(256)} %param.8) | copy-start | bytes 3076
where the time goes:
time: 437 us; the launch traced here: 436 us
  Pallas kernels  402 us (92%)
  local copies, waits for them, and re-layouts  22.8 us (5%)
  matrix products  6.95 us (2%)
    pallas_call x1, Pallas kernels, per_device(): pl.pallas_call(functools.partial(kernel, dims), name='reshard_experts', o...  402 us
    unnamed x5, local copies, waits for them, and re-layouts  22 us

commit v1 on v0

v1 whole, which is shorter than its diff:
```python
import functools

import jax
import jax.numpy as jnp
from jax import lax
from jax.experimental import pallas as pl
from jax.experimental.pallas import tpu as pltpu
from jax.sharding import PartitionSpec as P

EPS = 1e-06
GROUP = 8
MESH = pl.DeviceIdType.MESH
SLOTS = 4
PIECES = 6
EARLY = 2


def kernel(
    dims, gain, routes, rw, prompt, gm, um, dm, g_out, u_out, d_out, ans, slot_out,
    stage, wb, x, w, pr_in, nq, tok, wsend, gb, hid, yr, ys,
    st_sem, zs, zr, vs, vr, tzs, tzr, wzs, wzr, txs, txr, tw_sem, ps, pr, rs, rr,
):
    gr, fs, tp, experts, rows, width, cap, depth, hidden_all, split = dims
    me_g, me_f, me_t = lax.axis_index("gr"), lax.axis_index("fs"), lax.axis_index("tp")
    bf16, f32 = jnp.bfloat16, jnp.float32
    local = experts // fs
    half = local // 2
    groups = experts // GROUP
    quarter = depth // tp
    total = fs * cap
    tokens = prompt.shape[0]
    tile = min(256, cap)
    sub = rows // split
    apart = sub % 128 == 0
    masters, outs = (gm, um, dm), (g_out, u_out, d_out)

    def fs_at(k):
        return lax.rem(me_f + k, fs)

    def fs_from(k):
        return lax.rem(me_f + fs - k, fs)

    def gr_at(j):
        return lax.rem(me_g + j, gr)

    def remote(src, dst, ssem, rsem, where):
        return pltpu.make_async_remote_copy(
            src_ref=src, dst_ref=dst, send_sem=ssem, recv_sem=rsem,
            device_id=where, device_id_type=MESH,
        )

    def matrix(s):
        return (0, 1, 0, 1, 2, 2)[s]

    def half_of(s):
        return (0, 0, 1, 1, 0, 1)[s]

    def parts(s):
        h = half_of(s)
        if s >= 4 and split > 1:
            n = max(1, local // 4)
            return [(q * n, n, q * n, h * sub, sub) for q in range(local // n)]
        return [(q * half, half, h * half, q * sub, sub) for q in range(split)]

    def region(s, g, f, q):
        _, n, e0, r0, nr = parts(s)[q]
        at = pl.multiple_of((g * fs + f) * rows + r0, nr)
        return outs[matrix(s)].at[pl.ds(e0, n), pl.ds(at, nr), :]

    def buffered(s, k, q):
        b0, n, _, _, _ = parts(s)[q]
        return wb.at[s, k - 1, pl.ds(b0, n)]

    barrier = pltpu.get_barrier_semaphore()
    for k in range(1, fs):
        pl.semaphore_signal(barrier, inc=1, device_id={"fs": fs_at(k)}, device_id_type=MESH)
    for j in range(1, gr):
        pl.semaphore_signal(barrier, inc=1, device_id={"gr": gr_at(j)}, device_id_type=MESH)
    for j in range(1, tp):
        pl.semaphore_signal(
            barrier, inc=1, device_id={"tp": lax.rem(me_t + j, tp)}, device_id_type=MESH
        )

    if fs == 4:
        odd, side = lax.rem(me_f, 2), lax.rem(me_t, 2)
        near, far = 1 + 2 * odd, 3 - 2 * odd
        sending = [
            jnp.where(side == 0, 2, near), jnp.where(side == 0, far, 2), jnp.where(side == 0, near, far)
        ]
        hearing = [2, 1, 3]
    else:
        sending = list(range(1, fs))
        hearing = sending
    items = [(s, k) for s in range(PIECES) for k in [0] + sending]

    def load(i):
        s, k = items[i]
        first = fs_at(k) * local
        slot = i % SLOTS
        if s >= 4 and split > 1:
            cuts = [(0, local, 0, half_of(s) * sub)]
        else:
            cuts = [(q * half, half, half_of(s) * half, q * sub) for q in range(split)]
        return [
            pltpu.make_async_copy(
                masters[matrix(s)].at[pl.ds(first + e0, n), pl.ds(r0, sub)],
                stage.at[slot, pl.ds(b0, n)], st_sem.at[slot, c],
            )
            for c, (b0, n, e0, r0) in enumerate(cuts)
        ]

    for i in range(SLOTS):
        for c in load(i):
            c.start()
    prompt_copy = pltpu.make_async_copy(prompt, pr_in, tw_sem.at[0])
    prompt_copy.start()
    square = (rows, rows)
    diagonal = lax.broadcasted_iota(jnp.int32, square, 0) == lax.broadcasted_iota(jnp.int32, square, 1)
    column = jnp.sum(jnp.where(diagonal, gain[...], 0.0), axis=1, keepdims=True)
    gb[...] = jnp.broadcast_to(column, gb.shape)
    pl.semaphore_wait(barrier, (fs - 1) + (gr - 1) + (tp - 1))

    def z_copy(s, k, q):
        return remote(
            buffered(s, k, q), region(s, me_g, me_f, q), zs.at[s, k, q], zr.at[s, k, q],
            {"fs": fs_at(k)},
        )

    def z_landed(s, k, q):
        f = fs_from(k)
        ref = region(s, me_g, f, q)
        return remote(ref, ref, zs.at[s, k, q], zr.at[s, k, q], {"fs": f})

    def v_copy(s, k, j, q):
        ref = region(s, me_g, fs_from(k), q)
        return remote(ref, ref, vs.at[s, k, j - 1, q], vr.at[s, k, j - 1, q], {"gr": gr_at(j)})

    def v_landed(s, k, j, q):
        g = lax.rem(me_g + gr - j, gr)
        ref = region(s, g, fs_from(k), q)
        return remote(ref, ref, vs.at[s, k, j - 1, q], vr.at[s, k, j - 1, q], {"gr": g})

    def send_gr(s, k):
        for q in range(len(parts(s))):
            for j in range(1, gr):
                v_copy(s, k, j, q).start()

    def forward(s, k):
        for q in range(len(parts(s))):
            z_landed(s, k, q).wait_recv()
            for j in range(1, gr):
                v_copy(s, k, j, q).start()

    def arrived_gr(s, k):
        for q in range(len(parts(s))):
            for j in range(1, gr):
                v_landed(s, k, j, q).wait_recv()

    def cast_item(i):
        s, k = items[i]
        m, h, slot = matrix(s), half_of(s), i % SLOTS
        own = isinstance(k, int) and k == 0
        for c in load(i):
            c.wait()
        base = (me_g * fs + me_f) * rows
        if s >= 4 and split > 1:
            cuts = [(0, local, 0, h * sub)]
        else:
            cuts = [(q * half, half, h * half, q * sub) for q in range(split)]
        for b0, n, e0, r0 in cuts:
            scale = None
            if m < 2:
                scale = jnp.concatenate([gb[pl.ds(r0, sub)]] * (width // 128), axis=1)

            def cast(e, carry, b0=b0, e0=e0, r0=r0, scale=scale):
                value = stage[slot, b0 + e]
                if scale is not None:
                    value = scale * value
                if own:
                    at = pl.multiple_of(base + r0, sub)
                    outs[m][e0 + e, pl.ds(at, sub), :] = value.astype(bf16)
                else:
                    wb[s, k - 1, b0 + e] = value.astype(bf16)
                return carry

            lax.fori_loop(0, n, cast, 0)
        if i + SLOTS < len(items):
            for c in load(i + SLOTS):
                c.start()
        if own:
            if s < 3:
                send_gr(s, 0)
        else:
            for q in range(len(parts(s))):
                z_copy(s, k, q).start()

    def x_block(f, t):
        return x.at[
            pl.ds(pl.multiple_of(f * cap, cap), cap),
            pl.ds(pl.multiple_of(t * quarter, quarter), quarter),
        ]

    def w_block(f):
        return w.at[:, pl.ds(pl.multiple_of(f * cap, cap), cap)]

    def tok_copy(k):
        dst = fs_at(k)
        return remote(tok.at[(dst * local) // GROUP], x_block(me_f, me_t), tzs.at[k], tzr.at[k], {"fs": dst})

    def w_copy(k):
        dst = fs_at(k)
        return remote(wsend.at[dst], w_block(me_f), wzs.at[k], wzr.at[k], {"fs": dst})

    def tx_copy(k, j):
        ref = x_block(fs_from(k), me_t)
        return remote(ref, ref, txs.at[k, j], txr.at[k, j], {"tp": lax.rem(me_t + j, tp)})

    def prepare():
        prompt_copy.wait()
        step = min(64, tokens)
        mine = pl.ds(pl.multiple_of(me_t * quarter, quarter), quarter)

        def norm(r, carry):
            at = pl.ds(pl.multiple_of(r * step, step), step)
            wide = pr_in[at, :].astype(f32)
            scale = lax.rsqrt(jnp.mean(wide * wide, axis=-1, keepdims=True) + EPS)
            nq[at, :] = (pr_in[at, mine].astype(f32) * scale).astype(bf16)
            return carry

        lax.fori_loop(0, tokens // step, norm, 0)
        first, second = routes[0:1, :], routes[1:2, :]
        pad = max(8, groups)
        low = GROUP * lax.broadcasted_iota(jnp.int32, (pad, tokens), 0)
        hits = jnp.logical_and(first >= low, first < low + GROUP)
        flat = (tokens, tokens)
        before = lax.broadcasted_iota(jnp.int32, flat, 0) < lax.broadcasted_iota(jnp.int32, flat, 1)
        counts = jnp.dot(
            jnp.where(hits, 1.0, 0.0).astype(bf16), jnp.where(before, 1.0, 0.0).astype(bf16),
            preferred_element_type=f32,
        )
        lead = (lax.broadcasted_iota(jnp.int32, (pad, tokens), 0) * cap).astype(f32)
        slot = jnp.sum(jnp.where(hits, counts + lead, 0.0), axis=0, keepdims=True).astype(jnp.int32)
        slot_out[...] = slot
        for g in range(groups):
            spots = lax.broadcasted_iota(jnp.int32, (cap, tokens), 0) + g * cap
            place = jnp.where(spots == slot, 1.0, 0.0).astype(bf16)
            packed = jnp.dot(place, nq[...], preferred_element_type=f32).astype(bf16)
            tok[g] = packed

            @pl.when((me_f * local) // GROUP == g)
            def _(packed=packed):
                x[pl.ds(pl.multiple_of(me_f * cap, cap), cap), mine] = packed

            for d in range(fs):
                if (d * local) // GROUP != g:
                    continue
                named = lax.broadcasted_iota(jnp.int32, (w.shape[0], tokens), 0) + d * local
                spread = jnp.where(first == named, rw[0:1, :], 0.0)
                spread += jnp.where(second == named, rw[1:2, :], 0.0)
                packed_w = jnp.zeros((w.shape[0], cap), f32)
                for _ in range(3):
                    top = spread.astype(bf16)
                    packed_w += lax.dot_general(
                        top, place, (((1,), (1,)), ((), ())), preferred_element_type=f32
                    )
                    spread = spread - top.astype(f32)
                wsend[d] = packed_w

                @pl.when(me_f == d)
                def _(packed_w=packed_w):
                    w[:, pl.ds(pl.multiple_of(me_f * cap, cap), cap)] = packed_w

        for k in range(1, fs):
            tok_copy(k).start()
            w_copy(k).start()
        for j in range(1, tp):
            tx_copy(0, j).start()

    per = len(items) // PIECES
    for i in range(EARLY * per):
        cast_item(i)
    prepare()
    for i in range(EARLY * per, len(items)):
        cast_item(i)

    def tokens_on(k):
        f = fs_from(k)
        remote(x_block(f, me_t), x_block(f, me_t), tzs.at[k], tzr.at[k], {"fs": f}).wait_recv()
        remote(w_block(f), w_block(f), wzs.at[k], wzr.at[k], {"fs": f}).wait_recv()
        for j in range(1, tp):
            tx_copy(k, j).start()

    def tokens_here():
        for k in range(fs):
            f = fs_from(k)
            for j in range(1, tp):
                t = lax.rem(me_t + tp - j, tp)
                remote(x_block(f, t), x_block(f, t), txs.at[k, j], txr.at[k, j], {"tp": t}).wait_recv()

    def experts_of(h, todo):
        def one(n, carry):
            for i, act in enumerate(todo):
                pl.when(n == i * half // len(todo))(act)
            e = h * half + n

            def block(r, carry):
                at = pl.ds(pl.multiple_of(r * tile, tile), tile)
                xs = x[at, :]
                pre_gate = jnp.dot(xs, g_out[e], preferred_element_type=f32) * depth ** (-0.5)
                pre_up = jnp.dot(xs, u_out[e], preferred_element_type=f32) * depth ** (-0.5)
                ws = jnp.transpose(w[:, at])
                lane = lax.broadcasted_iota(jnp.int32, ws.shape, 1)
                weight = jnp.sum(jnp.where(lane == e, ws, 0.0), axis=1, keepdims=True)
                value = pre_gate / (1.0 + jnp.exp(-pre_gate)) * pre_up * weight
                hid[e, at, :] = value.astype(bf16)
                return carry

            lax.fori_loop(0, total // tile, block, 0)
            return carry

        lax.fori_loop(0, half, one, 0)

    size = sub if apart else max(128, rows)
    per_owner = quarter // size
    blocks = []

    def partial_copy(ci):
        at, owner, p, slot_of, _ = blocks[ci]
        return remote(
            x.at[:, pl.ds(at, size)],
            yr.at[slot_of, :, pl.ds(pl.multiple_of(p * size, size), size)],
            ps.at[ci], pr.at[slot_of, p], {"tp": owner},
        )

    def compute(ats):
        ats = [pl.multiple_of(at, size) for at in ats]

        def block(r, carry):
            here = pl.ds(pl.multiple_of(r * tile, tile), tile)
            acc = jnp.zeros((tile, size * len(ats)), f32)
            for e in range(local):
                cols = [d_out[e, pl.ds(at, size), :] for at in ats]
                cols = cols[0] if len(cols) == 1 else jnp.concatenate(cols, axis=0)
                acc += lax.dot_general(
                    hid[e, here, :], cols, (((1,), (1,)), ((), ())), preferred_element_type=f32
                )
            acc = (acc * hidden_all ** (-0.5)).astype(bf16)
            for n, at in enumerate(ats):
                x[here, pl.ds(at, size)] = acc[:, n * size : (n + 1) * size]
            return carry

        lax.fori_loop(0, total // tile, block, 0)
        for at in ats:
            owner = at // quarter
            turn = lax.rem(me_t + tp - owner, tp)
            ci = len(blocks)
            blocks.append((at, owner, lax.rem(at, quarter) // size, lax.rem(turn + tp - 1, tp), turn != 0))

            @pl.when(turn != 0)
            def _(ci=ci):
                partial_copy(ci).start()

    def part(p):
        return pl.ds(pl.multiple_of(p * size, size), size)

    def answer_copy(k, p):
        f = fs_at(k)
        at = pl.ds(pl.multiple_of(f * cap, cap), cap)
        return remote(
            ys.at[at, part(p)], ans.at[me_f, :, part(p)], rs.at[k, p], rr.at[k, p], {"fs": f}
        )

    def finish(ci):
        here, owner, p, _, away = blocks[ci]

        @pl.when(jnp.logical_not(away))
        def _():
            for j in range(1, tp):
                ref = yr.at[j - 1, :, part(p)]
                remote(
                    ref, ref, ps.at[ci], pr.at[j - 1, p], {"tp": lax.rem(me_t + j, tp)}
                ).wait_recv()
            for k in list(range(1, fs)) + [0]:
                at = pl.ds(pl.multiple_of(fs_at(k) * cap, cap), cap)
                value = x[at, pl.ds(here, size)].astype(f32)
                for j in range(tp - 1):
                    value += yr[j, at, part(p)].astype(f32)
                if k > 0:
                    ys[at, part(p)] = value.astype(bf16)
                    answer_copy(k, p).start()
                else:
                    ans[me_f, :, part(p)] = value.astype(bf16)

    def act(f, *args):
        return lambda: f(*args)

    for s in (0, 1):
        for k in hearing:
            forward(s, k)
    for k in range(1, fs):
        tokens_on(k)
    send_gr(3, 0)
    tokens_here()
    for s in (0, 1):
        for k in range(fs):
            arrived_gr(s, k)
    experts_of(0, [act(forward, 2, k) for k in hearing])
    send_gr(4, 0)
    for k in hearing:
        forward(3, k)
    send_gr(5, 0)
    for s in (2, 3):
        for k in range(fs):
            arrived_gr(s, k)
    experts_of(1, [act(forward, 4, k) for k in hearing])
    for k in range(fs):
        for j in range(1, tp):
            tx_copy(k, j).wait_send()
    if apart:
        def pair(r, k):
            arrived_gr(4 + r, k)
            compute([(g * fs + fs_from(k)) * rows + r * sub for g in range(gr)])

        done = 0
        for r in range(split):
            order = [0] + hearing
            for n, k in enumerate(order):
                if r == split - 1 and k != 0:
                    forward(5, k)
                pair(r, k)
                while done < len(blocks) - gr:
                    finish(done)
                    done += 1
        while done < len(blocks):
            finish(done)
            done += 1
    else:
        for k in hearing:
            forward(5, k)
        for s in (4, 5):
            for k in range(fs):
                arrived_gr(s, k)
        for index in range(depth // size):
            compute([jnp.int32(index * size)])
            if index >= 1:
                finish(index - 1)
        finish(len(blocks) - 1)

    for p in range(per_owner):
        for k in range(1, fs):
            answer_copy(k, p).wait_send()
            f = fs_from(k)
            ref = ans.at[f, :, part(p)]
            remote(ref, ref, rs.at[k, p], rr.at[k, p], {"fs": f}).wait_recv()
    for k in range(1, fs):
        tok_copy(k).wait_send()
        w_copy(k).wait_send()
    for s in range(PIECES):
        for q in range(len(parts(s))):
            for k in range(fs):
                if k > 0:
                    z_copy(s, k, q).wait_send()
                for j in range(1, gr):
                    v_copy(s, k, j, q).wait_send()
    for ci in range(len(blocks)):
        @pl.when(blocks[ci][4])
        def _(ci=ci):
            partial_copy(ci).wait_send()


def place_kernel(dims, g_in, u_in, d_in, ans, slot, g_out, u_out, d_out, blended, sems):
    groups, fs, cap, tokens = dims
    f32, bf16 = jnp.float32, jnp.bfloat16
    pairs = ((g_in, g_out), (u_in, u_out), (d_in, d_out))

    def copies():
        return [
            pltpu.make_async_copy(a.at[e], b.at[e], sems.at[m, e])
            for m, (a, b) in enumerate(pairs)
            for e in range(a.shape[0])
        ]

    for c in copies():
        c.start()
    flat = (tokens, tokens)
    diagonal = lax.broadcasted_iota(jnp.int32, flat, 0) == lax.broadcasted_iota(jnp.int32, flat, 1)
    column = jnp.sum(jnp.where(diagonal, slot[...].astype(f32), 0.0), axis=1, keepdims=True)
    column = column.astype(jnp.int32)
    total = jnp.zeros(blended.shape, f32)
    each = fs // groups
    for g in range(groups):
        spots = lax.broadcasted_iota(jnp.int32, (tokens, cap), 1) + g * cap
        back = jnp.where(spots == column, 1.0, 0.0).astype(bf16)
        value = ans[g * each]
        if each > 1:
            value = value.astype(f32)
            for n in range(1, each):
                value += ans[g * each + n].astype(f32)
            value = value.astype(bf16)
        total += jnp.dot(back, value, preferred_element_type=f32)
    blended[...] = total.astype(bf16)
    for c in copies():
        c.wait()


def per_device(prompt, norm_gain, gate_master, up_master, down_master, routes, route_weights):
    gr, fs, tp = lax.axis_size("gr"), lax.axis_size("fs"), lax.axis_size("tp")
    experts, rows, width = gate_master.shape
    tokens, depth = prompt.shape
    local = experts // fs
    half = local // 2
    groups = experts // GROUP
    cap = tokens // 2
    quarter = depth // tp
    total = fs * cap
    split = 2 if rows % 256 == 0 else 1
    sub = rows // split
    size = sub if sub % 128 == 0 else max(128, rows)
    per_owner = quarter // size
    wide = max(8, local)
    bf16, f32 = jnp.bfloat16, jnp.float32
    dims = (gr, fs, tp, experts, rows, width, cap, depth, width * tp, split)
    any_spec = pl.BlockSpec(memory_space=pl.ANY)
    vmem_spec = pl.BlockSpec(memory_space=pltpu.VMEM)
    ready = (local, gr * fs * rows, width)
    dma = pltpu.SemaphoreType.DMA
    vmem = pltpu.VMEM
    n_parts = max(4, split)
    landed = 2 * (3 * ready[0] * ready[1] * ready[2] + fs * cap * quarter)
    gate_here, up_here, down_here, answers, slot = pl.pallas_call(
        functools.partial(kernel, dims),
        name="reshard_experts",
        out_shape=(
            vmem(ready, bf16), vmem(ready, bf16), vmem(ready, bf16),
            vmem((fs, cap, quarter), bf16), vmem((1, tokens), jnp.int32),
        ),
        in_specs=[vmem_spec] * 3 + [any_spec] * 4,
        out_specs=(vmem_spec,) * 5,
        scratch_shapes=[
            vmem((SLOTS, half * split, sub, width), f32),
            vmem((PIECES, fs - 1, half * split, sub, width), bf16),
            vmem((total, depth), bf16),
            vmem((wide, total), f32),
            vmem((tokens, depth), bf16),
            vmem((tokens, quarter), bf16),
            vmem((groups, cap, quarter), bf16),
            vmem((fs, wide, cap), f32),
            vmem((rows, 128), f32),
            vmem((local, total, width), bf16),
            vmem((tp - 1, total, quarter), bf16),
            vmem((total, quarter), bf16),
            dma((SLOTS, split)),
            dma((PIECES, fs, n_parts)), dma((PIECES, fs, n_parts)),
            dma((PIECES, fs, gr - 1, n_parts)), dma((PIECES, fs, gr - 1, n_parts)),
            dma((fs,)), dma((fs,)), dma((fs,)), dma((fs,)),
            dma((fs, tp)), dma((fs, tp)),
            dma((2,)),
            dma((tp * per_owner,)), dma((tp - 1, per_owner)),
            dma((fs, per_owner)), dma((fs, per_owner)),
        ],
        compiler_params=pltpu.CompilerParams(
            collective_id=0, has_side_effects=True, vmem_limit_bytes=66000000 - landed
        ),
    )(norm_gain[None, :], routes.T, route_weights.T, prompt, gate_master, up_master, down_master)
    out = jax.ShapeDtypeStruct(ready, bf16)
    return pl.pallas_call(
        functools.partial(place_kernel, (groups, fs, cap, tokens)),
        name="place_outputs",
        out_shape=(out, out, out, jax.ShapeDtypeStruct((tokens, quarter), bf16)),
        in_specs=[vmem_spec] * 5,
        out_specs=(any_spec, any_spec, any_spec, vmem_spec),
        scratch_shapes=[dma((3, local))],
        compiler_params=pltpu.CompilerParams(vmem_limit_bytes=12000000),
    )(gate_here, up_here, down_here, answers, slot)


def solution(mesh):
    both = ("gr", "fs")
    in_specs = (
        P(both, None),
        P(both),
        P(None, both, "tp"),
        P(None, both, "tp"),
        P(None, both, "tp"),
        P(both, None),
        P(both, None),
    )
    out_specs = (
        P("fs", None, "tp"),
        P("fs", None, "tp"),
        P("fs", None, "tp"),
        P(both, "tp"),
    )
    return jax.shard_map(
        per_device, mesh=mesh, in_specs=in_specs, out_specs=out_specs, check_vma=False
    )
```

time: 437 us -> 407 us (0.931)
  local copies, waits for them, and re-layouts: 22.8 us -> 0 us
  matrix products: 6.95 us -> 0 us
    unnamed x5 -> x0, local copies, waits for them, and re-layouts: 22 us -> none
    pallas_call x0 -> x1, Pallas kernels: none -> 9.42 us  [per_device(): pl.pallas_call(functools.partial(place_kernel, (groups, fs, cap, tokens))...]
    pallas_call x1, Pallas kernels: 402 us -> 394 us  [per_device(): pl.pallas_call(functools.partial(kernel, dims), name='reshard_experts', o...]
    dot_general x4 -> x0, matrix products: 6.95 us -> none  [the longest x1 2.81 us: per_device(): jnp.dot(place.astype(bf16), normed, preferred_element_type=f32).astype(bf16)]
where the time goes in v1:
time: 407 us; the launch traced here: 404 us
  Pallas kernels  403 us (99%)
    pallas_call x1, Pallas kernels, per_device(): pl.pallas_call(functools.partial(kernel, dims), name='reshard_experts', o...  394 us
    pallas_call x1, Pallas kernels, per_device(): pl.pallas_call(functools.partial(place_kernel, (groups, fs, cap, tokens))...  9.42 us

profile of v1, /device:TPU:13, one launch (start us, length us, event | category | flops | bytes accessed | tf_op | source)
XLA Modules:
  0.0 403.7 jit_solution(742470555062009814)
XLA Ops:
  0.6 393.6 %reshard_experts.1 = (bf16[8,2048,256]{2,1,0:T(8,128)(2,1)S(1)}, bf16[8,2048,256]{2,1,0:T(8,128)(2,1)S(1)}, bf16[8,2048,256]{2,1,0:T(8,128)(2,1)S(1)}, bf16[4,256,512]{2,1,0:T(8,128)(2,1)S(1)}, s32[1,512]{1,0:T(1,128)S(1)}) custom-call(f32[1,256]{1,0:T(1,128)} %bitcast.5, s32[2,512]{1,0:T(2,128)} %bitcast.3, f32[2,512]{1,0:T(2,128)} %bitcast.4, ...), custom_call_target="tpu_custom_call" | custom-call | tf_op jit(solution)/shard_map/reshard_experts/pallas_call | solution.py:530
  394.3 9.4 %place_outputs.1 = (bf16[8,2048,256]{2,1,0:T(8,128)(2,1)}, bf16[8,2048,256]{2,1,0:T(8,128)(2,1)}, bf16[8,2048,256]{2,1,0:T(8,128)(2,1)}, bf16[512,512]{1,0:T(8,128)(2,1)}) custom-call(bf16[8,2048,256]{2,1,0:T(8,128)(2,1)S(1)} %get-tuple-element.9.g_in, bf16[8,2048,256]{2,1,0:T(8,128)(2,1)S(1)} %get-tuple-element.10.u_in, ...), custom_call_target="tpu_custom_call" | custom-call | tf_op jit(solution)/shard_map/place_outputs/pallas_call | solution.py:566

commit v2 on v1

--- a/solution.py
+++ b/solution.py
@@ -12,7 +12,7 @@
 MESH = pl.DeviceIdType.MESH
 SLOTS = 4
 PIECES = 6
-EARLY = 2
+EARLY = 1
 
 
 def kernel(
@@ -82,15 +82,16 @@
         )
 
     if fs == 4:
-        odd, side = lax.rem(me_f, 2), lax.rem(me_t, 2)
-        near, far = 1 + 2 * odd, 3 - 2 * odd
-        sending = [
-            jnp.where(side == 0, 2, near), jnp.where(side == 0, far, 2), jnp.where(side == 0, near, far)
-        ]
-        hearing = [2, 1, 3]
+        ahead = 1 + 2 * (me_f // 2)
+        sending = [ahead, 2, 4 - ahead]
+        beside, across = 3 - 2 * lax.rem(me_f, 2), 1 + (me_f + 1) // 2
+        fast, slow = [beside, across], [6 - beside - across]
+        inner = jnp.logical_and(me_f > 0, me_f < fs - 1)
     else:
         sending = list(range(1, fs))
-        hearing = sending
+        fast, slow = sending[:-1], sending[-1:]
+        inner = me_f >= 0
+        across = fs - 1
     items = [(s, k) for s in range(PIECES) for k in [0] + sending]
 
     def load(i):
@@ -140,13 +141,21 @@
         ref = region(s, g, fs_from(k), q)
         return remote(ref, ref, vs.at[s, k, j - 1, q], vr.at[s, k, j - 1, q], {"gr": g})
 
+    def z_send(s, k):
+        for q in range(len(parts(s))):
+            z_copy(s, k, q).start()
+
+    def z_sends(s):
+        for k in sending:
+            z_send(s, k)
+
     def send_gr(s, k):
         for q in range(len(parts(s))):
             for j in range(1, gr):
                 v_copy(s, k, j, q).start()
 
-    def forward(s, k):
-        for q in range(len(parts(s))):
+    def forward(s, k, only=None):
+        for q in range(len(parts(s))) if only is None else [only]:
             z_landed(s, k, q).wait_recv()
             for j in range(1, gr):
                 v_copy(s, k, j, q).start()
@@ -188,11 +197,12 @@
             for c in load(i + SLOTS):
                 c.start()
         if own:
-            if s < 3:
+            if s < 4:
                 send_gr(s, 0)
+        elif s < 4:
+            z_send(s, k)
         else:
-            for q in range(len(parts(s))):
-                z_copy(s, k, q).start()
+            pl.when(inner)(lambda: z_send(s, k))
 
     def x_block(f, t):
         return x.at[
@@ -300,7 +310,7 @@
     def experts_of(h, todo):
         def one(n, carry):
             for i, act in enumerate(todo):
-                pl.when(n == i * half // len(todo))(act)
+                pl.when(n == (i + 1) * half // (len(todo) + 1))(act)
             e = h * half + n
 
             def block(r, carry):
@@ -324,41 +334,43 @@
     per_owner = quarter // size
     blocks = []
 
-    def partial_copy(ci):
+    def partial_copy(ci, f):
         at, owner, p, slot_of, _ = blocks[ci]
+        here = pl.ds(pl.multiple_of(f * cap, cap), cap)
         return remote(
-            x.at[:, pl.ds(at, size)],
-            yr.at[slot_of, :, pl.ds(pl.multiple_of(p * size, size), size)],
-            ps.at[ci], pr.at[slot_of, p], {"tp": owner},
+            x.at[here, pl.ds(at, size)],
+            yr.at[slot_of, here, pl.ds(pl.multiple_of(p * size, size), size)],
+            ps.at[ci, f], pr.at[slot_of, p, f], {"tp": owner},
         )
 
     def compute(ats):
         ats = [pl.multiple_of(at, size) for at in ats]
 
-        def block(r, carry):
-            here = pl.ds(pl.multiple_of(r * tile, tile), tile)
-            acc = jnp.zeros((tile, size * len(ats)), f32)
-            for e in range(local):
-                cols = [d_out[e, pl.ds(at, size), :] for at in ats]
-                cols = cols[0] if len(cols) == 1 else jnp.concatenate(cols, axis=0)
-                acc += lax.dot_general(
-                    hid[e, here, :], cols, (((1,), (1,)), ((), ())), preferred_element_type=f32
-                )
-            acc = (acc * hidden_all ** (-0.5)).astype(bf16)
-            for n, at in enumerate(ats):
-                x[here, pl.ds(at, size)] = acc[:, n * size : (n + 1) * size]
-            return carry
-
-        lax.fori_loop(0, total // tile, block, 0)
+        mine = list(range(len(blocks), len(blocks) + len(ats)))
         for at in ats:
             owner = at // quarter
             turn = lax.rem(me_t + tp - owner, tp)
-            ci = len(blocks)
             blocks.append((at, owner, lax.rem(at, quarter) // size, lax.rem(turn + tp - 1, tp), turn != 0))
 
-            @pl.when(turn != 0)
-            def _(ci=ci):
-                partial_copy(ci).start()
+        def block(i, carry):
+            f = fs_at(i + 1)
+            for step in range(cap // tile):
+                here = pl.ds(pl.multiple_of(f * cap + step * tile, tile), tile)
+                acc = jnp.zeros((tile, size * len(ats)), f32)
+                for e in range(local):
+                    cols = [d_out[e, pl.ds(at, size), :] for at in ats]
+                    cols = cols[0] if len(cols) == 1 else jnp.concatenate(cols, axis=0)
+                    acc += lax.dot_general(
+                        hid[e, here, :], cols, (((1,), (1,)), ((), ())), preferred_element_type=f32
+                    )
+                acc = (acc * hidden_all ** (-0.5)).astype(bf16)
+                for n, at in enumerate(ats):
+                    x[here, pl.ds(at, size)] = acc[:, n * size : (n + 1) * size]
+            for ci in mine:
+                pl.when(blocks[ci][4])(lambda ci=ci: partial_copy(ci, f).start())
+            return carry
+
+        lax.fori_loop(0, fs, block, 0)
 
     def part(p):
         return pl.ds(pl.multiple_of(p * size, size), size)
@@ -375,13 +387,14 @@
 
         @pl.when(jnp.logical_not(away))
         def _():
-            for j in range(1, tp):
-                ref = yr.at[j - 1, :, part(p)]
-                remote(
-                    ref, ref, ps.at[ci], pr.at[j - 1, p], {"tp": lax.rem(me_t + j, tp)}
-                ).wait_recv()
             for k in list(range(1, fs)) + [0]:
-                at = pl.ds(pl.multiple_of(fs_at(k) * cap, cap), cap)
+                f = fs_at(k)
+                at = pl.ds(pl.multiple_of(f * cap, cap), cap)
+                for j in range(1, tp):
+                    ref = yr.at[j - 1, at, part(p)]
+                    remote(
+                        ref, ref, ps.at[ci, f], pr.at[j - 1, p, f], {"tp": lax.rem(me_t + j, tp)}
+                    ).wait_recv()
                 value = x[at, pl.ds(here, size)].astype(f32)
                 for j in range(tp - 1):
                     value += yr[j, at, part(p)].astype(f32)
@@ -394,25 +407,53 @@
     def act(f, *args):
         return lambda: f(*args)
 
-    for s in (0, 1):
-        for k in hearing:
+    def forwards(s, ks):
+        for k in ks:
             forward(s, k)
-    for k in range(1, fs):
+
+    def arrived(*steps):
+        for s in steps:
+            for k in range(fs):
+                arrived_gr(s, k)
+
+    forwards(0, fast)
+    for k in fast:
         tokens_on(k)
-    send_gr(3, 0)
+    forwards(0, slow)
+    forwards(1, fast)
+    for k in slow:
+        tokens_on(k)
+    forwards(2, fast)
+    send_gr(4, 0)
+    forwards(3, fast)
+    send_gr(5, 0)
+    outer = jnp.logical_not(inner)
+    forwards(1, slow)
+    forwards(2, slow)
     tokens_here()
-    for s in (0, 1):
-        for k in range(fs):
-            arrived_gr(s, k)
-    experts_of(0, [act(forward, 2, k) for k in hearing])
-    send_gr(4, 0)
-    for k in hearing:
-        forward(3, k)
-    send_gr(5, 0)
-    for s in (2, 3):
-        for k in range(fs):
-            arrived_gr(s, k)
-    experts_of(1, [act(forward, 4, k) for k in hearing])
+    arrived(0, 1)
+    experts_of(0, [])
+    forwards(3, slow)
+    arrived(2, 3)
+
+    def release(s):
+        @pl.when(outer)
+        def _():
+            for k in slow:
+                forward(s, k, 0)
+            z_sends(s)
+
+    def rest(s, k):
+        for q in range(1, len(parts(s))):
+            forward(s, k, q)
+
+    if fs == 4:
+        soon = [jnp.where(inner, slow[0], beside), jnp.where(inner, beside, slow[0])]
+    else:
+        soon = list(range(1, fs - 1))
+    late = across
+
+    experts_of(1, [act(forward, 4, soon[0]), act(release, 4)])
     for k in range(fs):
         for j in range(1, tp):
             tx_copy(k, j).wait_send()
@@ -421,22 +462,51 @@
             arrived_gr(4 + r, k)
             compute([(g * fs + fs_from(k)) * rows + r * sub for g in range(gr)])
 
-        done = 0
-        for r in range(split):
-            order = [0] + hearing
-            for n, k in enumerate(order):
-                if r == split - 1 and k != 0:
-                    forward(5, k)
-                pair(r, k)
-                while done < len(blocks) - gr:
-                    finish(done)
-                    done += 1
-        while done < len(blocks):
-            finish(done)
-            done += 1
+        done = [0]
+
+        def finish_to(count):
+            while done[0] < count:
+                finish(done[0])
+                done[0] += 1
+
+        def step(r, k, lag=2 * gr):
+            pair(r, k)
+            finish_to(len(blocks) - lag)
+
+        count = len(parts(5))
+        step(0, 0)
+        pl.when(inner)(lambda: forward(4, soon[-1], 0))
+        rest(4, soon[-1])
+        for k in soon[1:-1]:
+            forward(4, k)
+        step(0, soon[0])
+        for q in range(count // 2):
+            forward(4, late, q)
+        for k in soon[1:]:
+            step(0, k)
+        for q in range(count // 2, count):
+            forward(4, late, q)
+        pl.when(outer)(lambda: forward(5, soon[0]))
+        step(0, late)
+        step(1, 0)
+        release(5)
+        pl.when(inner)(lambda: forward(5, soon[0]))
+        step(1, soon[0], gr)
+        pl.when(inner)(lambda: forward(5, soon[-1], 0))
+        rest(5, soon[-1])
+        for k in soon[1:-1]:
+            forward(5, k)
+        for q in range(count - 2):
+            forward(5, late, q)
+        for k in soon[1:]:
+            step(1, k, gr)
+        for q in range(count - 2, count):
+            forward(5, late, q)
+        step(1, late, gr)
+        finish_to(len(blocks))
     else:
-        for k in hearing:
-            forward(5, k)
+        forwards(4, soon[1:] + [late])
+        forwards(5, soon + [late])
         for s in (4, 5):
             for k in range(fs):
                 arrived_gr(s, k)
@@ -465,7 +535,8 @@
     for ci in range(len(blocks)):
         @pl.when(blocks[ci][4])
         def _(ci=ci):
-            partial_copy(ci).wait_send()
+            for f in range(fs):
+                partial_copy(ci, f).wait_send()
 
 
 def place_kernel(dims, g_in, u_in, d_in, ans, slot, g_out, u_out, d_out, blended, sems):
@@ -555,7 +626,7 @@
             dma((fs,)), dma((fs,)), dma((fs,)), dma((fs,)),
             dma((fs, tp)), dma((fs, tp)),
             dma((2,)),
-            dma((tp * per_owner,)), dma((tp - 1, per_owner)),
+            dma((tp * per_owner, fs)), dma((tp - 1, per_owner, fs)),
             dma((fs, per_owner)), dma((fs, per_owner)),
         ],
         compiler_params=pltpu.CompilerParams(

time: 407 us -> 340 us (0.84)
  Pallas kernels: 403 us -> 338 us
    pallas_call x1, Pallas kernels: 394 us -> 328 us  [per_device(): pl.pallas_call(functools.partial(kernel, dims), name='reshard_experts', o...]
where the time goes in v2:
time: 340 us; the launch traced here: 338 us
  Pallas kernels  338 us (99%)
    pallas_call x1, Pallas kernels, per_device(): pl.pallas_call(functools.partial(kernel, dims), name='reshard_experts', o...  328 us
    pallas_call x1, Pallas kernels, per_device(): pl.pallas_call(functools.partial(place_kernel, (groups, fs, cap, tokens))...  9.42 us

profile of v2, /device:TPU:13, one launch (start us, length us, event | category | flops | bytes accessed | tf_op | source)
XLA Modules:
  0.0 338.2 jit_solution(14915554535812114802)
XLA Ops:
  0.6 328.1 %reshard_experts.1 = (bf16[8,2048,256]{2,1,0:T(8,128)(2,1)S(1)}, bf16[8,2048,256]{2,1,0:T(8,128)(2,1)S(1)}, bf16[8,2048,256]{2,1,0:T(8,128)(2,1)S(1)}, bf16[4,256,512]{2,1,0:T(8,128)(2,1)S(1)}, s32[1,512]{1,0:T(1,128)S(1)}) custom-call(f32[1,256]{1,0:T(1,128)} %bitcast.5, s32[2,512]{1,0:T(2,128)} %bitcast.3, f32[2,512]{1,0:T(2,128)} %bitcast.4, ...), custom_call_target="tpu_custom_call" | custom-call | tf_op jit(solution)/shard_map/reshard_experts/pallas_call | solution.py:601
  328.8 9.4 %place_outputs.1 = (bf16[8,2048,256]{2,1,0:T(8,128)(2,1)}, bf16[8,2048,256]{2,1,0:T(8,128)(2,1)}, bf16[8,2048,256]{2,1,0:T(8,128)(2,1)}, bf16[512,512]{1,0:T(8,128)(2,1)}) custom-call(bf16[8,2048,256]{2,1,0:T(8,128)(2,1)S(1)} %get-tuple-element.9.g_in, bf16[8,2048,256]{2,1,0:T(8,128)(2,1)S(1)} %get-tuple-element.10.u_in, ...), custom_call_target="tpu_custom_call" | custom-call | tf_op jit(solution)/shard_map/place_outputs/pallas_call | solution.py:637

commit v3 on v2

--- a/solution.py
+++ b/solution.py
@@ -18,7 +18,7 @@
 def kernel(
     dims, gain, routes, rw, prompt, gm, um, dm, g_out, u_out, d_out, ans, slot_out,
     stage, wb, x, w, pr_in, nq, tok, wsend, gb, hid, yr, ys,
-    st_sem, zs, zr, vs, vr, tzs, tzr, wzs, wzr, txs, txr, tw_sem, ps, pr, rs, rr,
+    st_sem, zs, zr, zl, vs, vr, tzs, tzr, wzs, wzr, txs, txr, tw_sem, ps, pr, rs, rr,
 ):
     gr, fs, tp, experts, rows, width, cap, depth, hidden_all, split = dims
     me_g, me_f, me_t = lax.axis_index("gr"), lax.axis_index("fs"), lax.axis_index("tp")
@@ -121,25 +121,33 @@
     gb[...] = jnp.broadcast_to(column, gb.shape)
     pl.semaphore_wait(barrier, (fs - 1) + (gr - 1) + (tp - 1))
 
+    def z_sem(s, k, q):
+        return zl.at[s - 4, k - 1, q] if s >= 4 else zr.at[s, k - 1]
+
+    def piece(s, g, f):
+        h = half_of(s)
+        e0, n, r0, nr = (0, local, h * sub, sub) if s >= 4 and split > 1 else (h * half, half, 0, rows)
+        at = pl.multiple_of((g * fs + f) * rows + r0, nr)
+        return outs[matrix(s)].at[pl.ds(e0, n), pl.ds(at, nr), :]
+
     def z_copy(s, k, q):
         return remote(
-            buffered(s, k, q), region(s, me_g, me_f, q), zs.at[s, k, q], zr.at[s, k, q],
-            {"fs": fs_at(k)},
+            buffered(s, k, q), region(s, me_g, me_f, q), zs.at[s], z_sem(s, k, q), {"fs": fs_at(k)},
         )
 
     def z_landed(s, k, q):
         f = fs_from(k)
-        ref = region(s, me_g, f, q)
-        return remote(ref, ref, zs.at[s, k, q], zr.at[s, k, q], {"fs": f})
+        ref = piece(s, me_g, f) if s < 4 else region(s, me_g, f, q)
+        return remote(ref, ref, zs.at[s], z_sem(s, k, q), {"fs": f})
 
     def v_copy(s, k, j, q):
         ref = region(s, me_g, fs_from(k), q)
-        return remote(ref, ref, vs.at[s, k, j - 1, q], vr.at[s, k, j - 1, q], {"gr": gr_at(j)})
-
-    def v_landed(s, k, j, q):
+        return remote(ref, ref, vs.at[matrix(s), j - 1], vr.at[s, k, j - 1], {"gr": gr_at(j)})
+
+    def v_landed(s, k, j):
         g = lax.rem(me_g + gr - j, gr)
-        ref = region(s, g, fs_from(k), q)
-        return remote(ref, ref, vs.at[s, k, j - 1, q], vr.at[s, k, j - 1, q], {"gr": g})
+        ref = piece(s, g, fs_from(k))
+        return remote(ref, ref, vs.at[matrix(s), j - 1], vr.at[s, k, j - 1], {"gr": g})
 
     def z_send(s, k):
         for q in range(len(parts(s))):
@@ -156,14 +164,14 @@
 
     def forward(s, k, only=None):
         for q in range(len(parts(s))) if only is None else [only]:
-            z_landed(s, k, q).wait_recv()
+            if s >= 4 or q == 0:
+                z_landed(s, k, q).wait_recv()
             for j in range(1, gr):
                 v_copy(s, k, j, q).start()
 
     def arrived_gr(s, k):
-        for q in range(len(parts(s))):
-            for j in range(1, gr):
-                v_landed(s, k, j, q).wait_recv()
+        for j in range(1, gr):
+            v_landed(s, k, j).wait_recv()
 
     def cast_item(i):
         s, k = items[i]
@@ -223,7 +231,7 @@
 
     def tx_copy(k, j):
         ref = x_block(fs_from(k), me_t)
-        return remote(ref, ref, txs.at[k, j], txr.at[k, j], {"tp": lax.rem(me_t + j, tp)})
+        return remote(ref, ref, txs.at[j - 1], txr.at[k, j - 1], {"tp": lax.rem(me_t + j, tp)})
 
     def prepare():
         prompt_copy.wait()
@@ -305,7 +313,7 @@
             f = fs_from(k)
             for j in range(1, tp):
                 t = lax.rem(me_t + tp - j, tp)
-                remote(x_block(f, t), x_block(f, t), txs.at[k, j], txr.at[k, j], {"tp": t}).wait_recv()
+                remote(x_block(f, t), x_block(f, t), txs.at[j - 1], txr.at[k, j - 1], {"tp": t}).wait_recv()
 
     def experts_of(h, todo):
         def one(n, carry):
@@ -340,7 +348,7 @@
         return remote(
             x.at[here, pl.ds(at, size)],
             yr.at[slot_of, here, pl.ds(pl.multiple_of(p * size, size), size)],
-            ps.at[ci, f], pr.at[slot_of, p, f], {"tp": owner},
+            ps.at[ci], pr.at[slot_of, p, f], {"tp": owner},
         )
 
     def compute(ats):
@@ -379,8 +387,18 @@
         f = fs_at(k)
         at = pl.ds(pl.multiple_of(f * cap, cap), cap)
         return remote(
-            ys.at[at, part(p)], ans.at[me_f, :, part(p)], rs.at[k, p], rr.at[k, p], {"fs": f}
+            ys.at[at, part(p)], ans.at[me_f, :, part(p)], rs.at[k - 1], rr.at[k - 1], {"fs": f}
         )
+
+    held = [False]
+
+    def release_answers(count):
+        held[0] = False
+        for ci in range(count):
+            @pl.when(jnp.logical_not(blocks[ci][4]))
+            def _(ci=ci):
+                for k in range(1, fs):
+                    answer_copy(k, blocks[ci][2]).start()
 
     def finish(ci):
         here, owner, p, _, away = blocks[ci]
@@ -393,16 +411,37 @@
                 for j in range(1, tp):
                     ref = yr.at[j - 1, at, part(p)]
                     remote(
-                        ref, ref, ps.at[ci, f], pr.at[j - 1, p, f], {"tp": lax.rem(me_t + j, tp)}
+                        ref, ref, ps.at[ci], pr.at[j - 1, p, f], {"tp": lax.rem(me_t + j, tp)}
                     ).wait_recv()
                 value = x[at, pl.ds(here, size)].astype(f32)
                 for j in range(tp - 1):
                     value += yr[j, at, part(p)].astype(f32)
                 if k > 0:
                     ys[at, part(p)] = value.astype(bf16)
-                    answer_copy(k, p).start()
+                    if not held[0]:
+                        answer_copy(k, p).start()
                 else:
                     ans[me_f, :, part(p)] = value.astype(bf16)
+
+    def drain(steps, gathered=()):
+        for s in steps:
+            remote(wb.at[s], wb.at[s], zs.at[s], zr.at[0, 0], {"fs": fs_at(1)}).wait_send()
+        for m in gathered:
+            ref = outs[m].at[:, pl.ds(pl.multiple_of(me_g * fs * rows, rows), fs * rows), :]
+            for j in range(1, gr):
+                remote(ref, ref, vs.at[m, j - 1], vr.at[0, 0, j - 1], {"gr": gr_at(j)}).wait_send()
+        if 0 in steps:
+            for k in range(1, fs):
+                tok_copy(k).wait_send()
+                w_copy(k).wait_send()
+
+    def drain_partials(which):
+        for ci in which:
+            @pl.when(blocks[ci][4])
+            def _(ci=ci):
+                at, owner, p, slot_of, _ = blocks[ci]
+                ref = x.at[:, pl.ds(at, size)]
+                remote(ref, ref, ps.at[ci], pr.at[slot_of, p, 0], {"tp": owner}).wait_send()
 
     def act(f, *args):
         return lambda: f(*args)
@@ -441,7 +480,12 @@
         def _():
             for k in slow:
                 forward(s, k, 0)
-            z_sends(s)
+            if s == 4:
+                z_sends(4)
+                z_send(5, sending[0])
+            else:
+                for k in sending[:0:-1]:
+                    z_send(5, k)
 
     def rest(s, k):
         for q in range(1, len(parts(s))):
@@ -454,9 +498,9 @@
     late = across
 
     experts_of(1, [act(forward, 4, soon[0]), act(release, 4)])
-    for k in range(fs):
-        for j in range(1, tp):
-            tx_copy(k, j).wait_send()
+    for j in range(1, tp):
+        ref = x.at[:, pl.ds(pl.multiple_of(me_t * quarter, quarter), quarter)]
+        remote(ref, ref, txs.at[j - 1], txr.at[0, j - 1], {"tp": lax.rem(me_t + j, tp)}).wait_send()
     if apart:
         def pair(r, k):
             arrived_gr(4 + r, k)
@@ -474,12 +518,14 @@
             finish_to(len(blocks) - lag)
 
         count = len(parts(5))
+        held[0] = True
         step(0, 0)
         pl.when(inner)(lambda: forward(4, soon[-1], 0))
         rest(4, soon[-1])
         for k in soon[1:-1]:
             forward(4, k)
         step(0, soon[0])
+        drain([0, 1, 2, 3])
         for q in range(count // 2):
             forward(4, late, q)
         for k in soon[1:]:
@@ -492,17 +538,25 @@
         release(5)
         pl.when(inner)(lambda: forward(5, soon[0]))
         step(1, soon[0], gr)
-        pl.when(inner)(lambda: forward(5, soon[-1], 0))
-        rest(5, soon[-1])
-        for k in soon[1:-1]:
-            forward(5, k)
-        for q in range(count - 2):
-            forward(5, late, q)
-        for k in soon[1:]:
+        middle, final = soon[1:], late
+        if fs == 4:
+            middle, final = [jnp.where(inner, beside, across)], jnp.where(inner, across, slow[0])
+            pl.when(outer)(lambda: forward(5, slow[0], 1))
+        forwards(5, middle)
+        drain([4])
+        drain_partials(range(gr * fs))
+
+        @pl.when(inner)
+        def _():
+            for q in range(count - 2):
+                forward(5, final, q)
+
+        for k in middle:
             step(1, k, gr)
         for q in range(count - 2, count):
-            forward(5, late, q)
-        step(1, late, gr)
+            forward(5, final, q)
+        release_answers(done[0])
+        step(1, final, gr)
         finish_to(len(blocks))
     else:
         forwards(4, soon[1:] + [late])
@@ -516,30 +570,18 @@
                 finish(index - 1)
         finish(len(blocks) - 1)
 
-    for p in range(per_owner):
-        for k in range(1, fs):
-            answer_copy(k, p).wait_send()
-            f = fs_from(k)
-            ref = ans.at[f, :, part(p)]
-            remote(ref, ref, rs.at[k, p], rr.at[k, p], {"fs": f}).wait_recv()
     for k in range(1, fs):
-        tok_copy(k).wait_send()
-        w_copy(k).wait_send()
-    for s in range(PIECES):
-        for q in range(len(parts(s))):
-            for k in range(fs):
-                if k > 0:
-                    z_copy(s, k, q).wait_send()
-                for j in range(1, gr):
-                    v_copy(s, k, j, q).wait_send()
-    for ci in range(len(blocks)):
-        @pl.when(blocks[ci][4])
-        def _(ci=ci):
-            for f in range(fs):
-                partial_copy(ci, f).wait_send()
-
-
-def place_kernel(dims, g_in, u_in, d_in, ans, slot, g_out, u_out, d_out, blended, sems):
+        f = fs_at(k)
+        ref = ys.at[pl.ds(pl.multiple_of(f * cap, cap), cap), :]
+        remote(ref, ref, rs.at[k - 1], rr.at[k - 1], {"fs": f}).wait_send()
+    drain([5] if apart else range(PIECES), range(3))
+    drain_partials(range(gr * fs if apart else 0, len(blocks)))
+    for k in range(1, fs):
+        f = fs_from(k)
+        remote(ans.at[f], ans.at[f], rs.at[k - 1], rr.at[k - 1], {"fs": f}).wait_recv()
+
+
+def place_kernel(dims, g_in, u_in, d_in, ans, slot, g_out, u_out, d_out, blended, mixed, sems, mixed_sem):
     groups, fs, cap, tokens = dims
     f32, bf16 = jnp.float32, jnp.bfloat16
     pairs = ((g_in, g_out), (u_in, u_out), (d_in, d_out))
@@ -569,9 +611,12 @@
                 value += ans[g * each + n].astype(f32)
             value = value.astype(bf16)
         total += jnp.dot(back, value, preferred_element_type=f32)
-    blended[...] = total.astype(bf16)
+    mixed[...] = total.astype(bf16)
+    last = pltpu.make_async_copy(mixed, blended, mixed_sem)
+    last.start()
     for c in copies():
         c.wait()
+    last.wait()
 
 
 def per_device(prompt, norm_gain, gate_master, up_master, down_master, routes, route_weights):
@@ -621,13 +666,13 @@
             vmem((tp - 1, total, quarter), bf16),
             vmem((total, quarter), bf16),
             dma((SLOTS, split)),
-            dma((PIECES, fs, n_parts)), dma((PIECES, fs, n_parts)),
-            dma((PIECES, fs, gr - 1, n_parts)), dma((PIECES, fs, gr - 1, n_parts)),
+            dma((PIECES,)), dma((4, fs - 1)), dma((2, fs - 1, n_parts)),
+            dma((3, gr - 1)), dma((PIECES, fs, gr - 1)),
             dma((fs,)), dma((fs,)), dma((fs,)), dma((fs,)),
-            dma((fs, tp)), dma((fs, tp)),
-            dma((2,)),
-            dma((tp * per_owner, fs)), dma((tp - 1, per_owner, fs)),
-            dma((fs, per_owner)), dma((fs, per_owner)),
+            dma((tp - 1,)), dma((fs, tp - 1)),
+            dma((1,)),
+            dma((tp * per_owner,)), dma((tp - 1, per_owner, fs)),
+            dma((fs - 1,)), dma((fs - 1,)),
         ],
         compiler_params=pltpu.CompilerParams(
             collective_id=0, has_side_effects=True, vmem_limit_bytes=66000000 - landed
@@ -639,8 +684,8 @@
         name="place_outputs",
         out_shape=(out, out, out, jax.ShapeDtypeStruct((tokens, quarter), bf16)),
         in_specs=[vmem_spec] * 5,
-        out_specs=(any_spec, any_spec, any_spec, vmem_spec),
-        scratch_shapes=[dma((3, local))],
+        out_specs=(any_spec,) * 4,
+        scratch_shapes=[vmem((tokens, quarter), bf16), dma((3, local)), dma],
         compiler_params=pltpu.CompilerParams(vmem_limit_bytes=12000000),
     )(gate_here, up_here, down_here, answers, slot)
 

time: 340 us -> 333 us (0.979)
  Pallas kernels: 338 us -> 330 us
    pallas_call x1, Pallas kernels: 328 us -> 322 us  [per_device(): pl.pallas_call(functools.partial(kernel, dims), name='reshard_experts', o...]
where the time goes in v3:
time: 333 us; the launch traced here: 331 us
  Pallas kernels  330 us (99%)
    pallas_call x1, Pallas kernels, per_device(): pl.pallas_call(functools.partial(kernel, dims), name='reshard_experts', o...  322 us
    pallas_call x1, Pallas kernels, per_device(): pl.pallas_call(functools.partial(place_kernel, (groups, fs, cap, tokens))...  8.72 us

profile of v3, /device:TPU:13, one launch (start us, length us, event | category | flops | bytes accessed | tf_op | source)
XLA Modules:
  0.0 331.0 jit_solution(11592034802829542021)
XLA Ops:
  0.6 321.7 %reshard_experts.1 = (bf16[8,2048,256]{2,1,0:T(8,128)(2,1)S(1)}, bf16[8,2048,256]{2,1,0:T(8,128)(2,1)S(1)}, bf16[8,2048,256]{2,1,0:T(8,128)(2,1)S(1)}, bf16[4,256,512]{2,1,0:T(8,128)(2,1)S(1)}, s32[1,512]{1,0:T(1,128)S(1)}) custom-call(f32[1,256]{1,0:T(1,128)} %bitcast.5, s32[2,512]{1,0:T(2,128)} %bitcast.3, f32[2,512]{1,0:T(2,128)} %bitcast.4, ...), custom_call_target="tpu_custom_call" | custom-call | tf_op jit(solution)/shard_map/reshard_experts/pallas_call | solution.py:646
  322.3 8.7 %place_outputs.1 = (bf16[8,2048,256]{2,1,0:T(8,128)(2,1)}, bf16[8,2048,256]{2,1,0:T(8,128)(2,1)}, bf16[8,2048,256]{2,1,0:T(8,128)(2,1)}, bf16[512,512]{1,0:T(8,128)(2,1)}) custom-call(bf16[8,2048,256]{2,1,0:T(8,128)(2,1)S(1)} %get-tuple-element.9.g_in, bf16[8,2048,256]{2,1,0:T(8,128)(2,1)S(1)} %get-tuple-element.10.u_in, ...), custom_call_target="tpu_custom_call" | custom-call | tf_op jit(solution)/shard_map/place_outputs/pallas_call | solution.py:682
